TPU v7x, 32 devices: a whole 2x2x4 slice. The times are simulated.
32 devices in a mesh: sp: 8 (over z, y), tp: 4 (over x, core).
Axes of the slice: x: 2, y: 2, z: 4, core: 2. Of those that a mesh axis runs over, the one named last changes fastest.
Arguments:
- residual: bfloat16 [2048, 2048], P(('sp', 'tp')), may hold values from -6 to 6
- ssm_input: bfloat16 [2048, 2048], P('sp', 'tp'), may hold values from -6 to 6
- pole_real: float32 [128, 64], P('tp'), may hold values from -2 to 0
- pole_imaginary: float32 [128, 64], P('tp'), may hold values from 1 to 100
- step_log: float32 [128], P('tp'), may hold values from -8 to 0
- input_real: float32 [128, 64, 16], P('tp'), may hold values from -1 to 1
- entry_map_quadrature: float32 [128, 64, 16], P('tp'), may hold values from -1 to 1
- output_real: float32 [128, 16, 64], P('tp'), may hold values from -0.5 to 0.5
- output_imaginary: float32 [128, 16, 64], P('tp'), may hold values from -0.5 to 0.5
- added_log_decay: float32 [2048, 128], P('sp', 'tp'), may hold values from -2 to 0
- out_weight: bfloat16 [2048, 2048], P('tp'), may hold values from -0.125 to 0.125
- mix_gain: float32 [2048], replicated, may hold values from 0.1 to 1.9
- gate_weight: bfloat16 [2048, 5632], P('sp', 'tp'), may hold values from -0.125 to 0.125
- up_weight: bfloat16 [2048, 5632], P('sp', 'tp'), may hold values from -0.125 to 0.125
- down_weight: bfloat16 [2048, 5632], P('sp', 'tp'), may hold values from -0.078125 to 0.078125
- pre_gain: float32 [2048], replicated, may hold values from 0.1 to 1.9
- post_gain: float32 [2048], replicated, may hold values from 0.1 to 1.9
Outputs:
- merged: bfloat16 [2048, 2048], P(('sp', 'tp'))
All inputs are finite; a program needn't handle non-finite values.
Results may differ from a plain program's by a relative error of at most 0.017.
Values may be sent and summed in bfloat16 or wider, within the bound.
A program may use at most 128 MiB of HBM per device.

v0:
```python
import jax
import jax.numpy as jnp
from jax import lax
from jax.sharding import PartitionSpec as P

EXACT = lax.Precision.HIGHEST
EPSILON = 1e-06
SPAN_ROWS = 16


def carried_in(shard, axis, combine, identity):
    count, place = (lax.axis_size(axis), lax.axis_index(axis))
    everything = jax.tree.map(
        lambda part, kind: lax.all_gather(part.astype(kind), axis),
        shard,
        (jnp.bfloat16, jnp.bfloat16, jnp.bfloat16, jnp.bfloat16),
    )
    start = jax.tree.map(
        lambda part, zero: jnp.broadcast_to(jnp.asarray(zero, part.dtype), part.shape),
        shard,
        identity,
    )

    def step(k, before):
        reached = k < place
        new = combine(
            before, jax.tree.map(lambda part, own: part[k].astype(own.dtype), everything, shard)
        )
        return jax.tree.map(lambda a, b: jnp.where(reached, a, b), new, before)

    return lax.fori_loop(0, count, step, start)


def rms_scale(values, gain):
    return values * lax.rsqrt(jnp.mean(values * values, axis=-1, keepdims=True) + EPSILON) * gain


def round_half(values):
    return lax.optimization_barrier(values.astype(jnp.bfloat16))


def chain_link(earlier, later):
    decay_real, decay_imaginary, state_real, state_imaginary = earlier
    next_real, next_imaginary, drive_real, drive_imaginary = later
    return (
        next_real * decay_real - next_imaginary * decay_imaginary,
        next_real * decay_imaginary + next_imaginary * decay_real,
        next_real * state_real - next_imaginary * state_imaginary + drive_real,
        next_real * state_imaginary + next_imaginary * state_real + drive_imaginary,
    )


def blocked_scan(decay_real, decay_imaginary, drive_real, drive_imaginary):
    row_count, flat = decay_real.shape
    span_count = row_count // SPAN_ROWS
    shaped = [
        item.reshape(span_count, SPAN_ROWS, flat)
        for item in (decay_real, decay_imaginary, drive_real, drive_imaginary)
    ]
    current = tuple((item[:, 0] for item in shaped))
    collected = [current]
    for step in range(1, SPAN_ROWS):
        current = chain_link(current, tuple((item[:, step] for item in shaped)))
        collected.append(current)
    stacked = tuple((jnp.stack([entry[part] for entry in collected], axis=1) for part in range(4)))
    totals = tuple((item[:, -1] for item in stacked))
    inclusive = lax.associative_scan(chain_link, totals, axis=0)
    unit = jnp.ones((1, flat), jnp.float32)
    nothing = jnp.zeros((1, flat), jnp.float32)
    carry_pr = jnp.concatenate([unit, inclusive[0][:-1]], axis=0)[:, None]
    carry_pi = jnp.concatenate([nothing, inclusive[1][:-1]], axis=0)[:, None]
    carry_sr = jnp.concatenate([nothing, inclusive[2][:-1]], axis=0)[:, None]
    carry_si = jnp.concatenate([nothing, inclusive[3][:-1]], axis=0)[:, None]
    local_pr, local_pi, local_sr, local_si = stacked
    product_real = local_pr * carry_pr - local_pi * carry_pi
    product_imaginary = local_pr * carry_pi + local_pi * carry_pr
    state_real = local_sr + local_pr * carry_sr - local_pi * carry_si
    state_imaginary = local_si + local_pr * carry_si + local_pi * carry_sr
    return tuple(
        (
            item.reshape(row_count, flat)
            for item in (product_real, product_imaginary, state_real, state_imaginary)
        )
    )


def local_states(
    inputs, pole_real, pole_imaginary, step_log, input_real, entry_map_quadrature, added_log_decay
):
    row_count = inputs.shape[0]
    groups, hidden_states = pole_real.shape
    width = input_real.shape[2]
    flat = groups * hidden_states
    step_size = jnp.exp(step_log)[:, None]
    log_size = pole_real * step_size
    angle = pole_imaginary * step_size
    cosine = jnp.cos(angle)
    sine = jnp.sin(angle)
    lift_real = jnp.expm1(log_size) * cosine - 2.0 * jnp.sin(0.5 * angle) ** 2
    lift_imaginary = jnp.exp(log_size) * sine
    denominator = pole_real * pole_real + pole_imaginary * pole_imaginary
    ratio_real = (lift_real * pole_real + lift_imaginary * pole_imaginary) / denominator
    ratio_imaginary = (lift_imaginary * pole_real - lift_real * pole_imaginary) / denominator
    bar_real = (
        ratio_real[..., None] * input_real - ratio_imaginary[..., None] * entry_map_quadrature
    )
    bar_imaginary = (
        ratio_real[..., None] * entry_map_quadrature + ratio_imaginary[..., None] * input_real
    )
    identity = jnp.eye(groups, dtype=jnp.float32)
    entry_real = jnp.einsum("gnc,gh->gchn", bar_real, identity).reshape(groups * width, flat)
    entry_imaginary = jnp.einsum("gnc,gh->gchn", bar_imaginary, identity).reshape(
        groups * width, flat
    )
    entry = jnp.concatenate([entry_real, entry_imaginary], axis=1)
    drive = jnp.dot(inputs.astype(jnp.float32), entry, precision=EXACT)
    drive_real = drive[:, :flat]
    drive_imaginary = drive[:, flat:]
    pole_magnitude = jnp.exp(log_size[None] + added_log_decay[:, :, None])
    decay_real = (pole_magnitude * cosine[None]).reshape(row_count, flat)
    decay_imaginary = (pole_magnitude * sine[None]).reshape(row_count, flat)
    return blocked_scan(decay_real, decay_imaginary, drive_real, drive_imaginary)


def apply_carry(scanned, carry_real, carry_imaginary):
    product_real, product_imaginary, state_real, state_imaginary = scanned
    return (
        state_real + product_real * carry_real - product_imaginary * carry_imaginary,
        state_imaginary + product_real * carry_imaginary + product_imaginary * carry_real,
    )


def readout(state_real, state_imaginary, output_real, output_imaginary):
    groups, width, hidden_states = output_real.shape
    identity = jnp.eye(groups, dtype=jnp.float32)
    read_real = jnp.einsum("gcn,gh->gnhc", output_real, identity).reshape(
        groups * hidden_states, groups * width
    )
    read_imaginary = jnp.einsum("gcn,gh->gnhc", output_imaginary, identity).reshape(
        groups * hidden_states, groups * width
    )
    real_part = jnp.dot(state_real, read_real, precision=EXACT)
    other_part = jnp.dot(state_imaginary, read_imaginary, precision=EXACT)
    return jax.nn.gelu(real_part - other_part).astype(jnp.bfloat16)


def shards(
    residual,
    ssm_input,
    pole_real,
    pole_imaginary,
    step_log,
    input_real,
    entry_map_quadrature,
    output_real,
    output_imaginary,
    added_log_decay,
    out_weight,
    mix_gain,
    gate_weight,
    up_weight,
    down_weight,
    pre_gain,
    post_gain,
):
    scanned = local_states(
        ssm_input,
        pole_real,
        pole_imaginary,
        step_log,
        input_real,
        entry_map_quadrature,
        added_log_decay,
    )
    unit = jnp.ones_like(scanned[0][-1])
    nothing = jnp.zeros_like(scanned[0][-1])
    carry_in = carried_in(
        (scanned[0][-1], scanned[1][-1], scanned[2][-1], scanned[3][-1]),
        "sp",
        chain_link,
        (unit, nothing, nothing, nothing),
    )
    state_real, state_imaginary = apply_carry(scanned, carry_in[2], carry_in[3])
    activated = readout(state_real, state_imaginary, output_real, output_imaginary)
    block = activated
    mixed_own = lax.psum_scatter(
        jnp.dot(block, out_weight, preferred_element_type=jnp.float32).astype(jnp.bfloat16),
        "tp",
        scatter_dimension=0,
        tiled=True,
    ).astype(jnp.float32)
    middle_local_part = round_half(residual.astype(jnp.float32) + rms_scale(mixed_own, mix_gain))
    normed_own = rms_scale(middle_local_part.astype(jnp.float32), pre_gain).astype(jnp.bfloat16)
    mixer_input = lax.all_gather(normed_own, "tp", axis=0, tiled=True)
    gate_full, up_full, down_full = (
        lax.all_gather(gate_weight, "sp", axis=0, tiled=True),
        lax.all_gather(up_weight, "sp", axis=0, tiled=True),
        lax.all_gather(down_weight, "sp", axis=0, tiled=True),
    )
    gate_act = jnp.dot(mixer_input, gate_full, preferred_element_type=jnp.float32)
    up_act = jnp.dot(mixer_input, up_full, preferred_element_type=jnp.float32)
    hidden = (jax.nn.silu(gate_act) * up_act).astype(jnp.bfloat16)
    block = hidden
    mixer_own = lax.psum_scatter(
        lax.dot_general(
            block, down_full, (((1,), (1,)), ((), ())), preferred_element_type=jnp.float32
        ).astype(jnp.bfloat16),
        "tp",
        scatter_dimension=0,
        tiled=True,
    ).astype(jnp.float32)
    merged = middle_local_part.astype(jnp.float32) + 0.5 * rms_scale(mixer_own, post_gain)
    return merged.astype(jnp.bfloat16)


def solution(mesh):
    return jax.shard_map(
        shards,
        mesh=mesh,
        in_specs=(
            P(("sp", "tp"), None),
            P("sp", "tp"),
            P("tp", None),
            P("tp", None),
            P("tp"),
            P("tp", None, None),
            P("tp", None, None),
            P("tp", None, None),
            P("tp", None, None),
            P("sp", "tp"),
            P("tp", None),
            P(),
            P("sp", "tp"),
            P("sp", "tp"),
            P("sp", "tp"),
            P(),
            P(),
        ),
        out_specs=P(("sp", "tp"), None),
        check_vma=False,
    )
```

profile of v0, /device:TPU:0, one launch (start us, length us, event | category | flops | bytes accessed | tf_op | source)
XLA Modules:
  0.0 810.7 jit_solution(13676780380514145849)
XLA Ops:
  9.5 8.4 %multiply_bitcast_fusion.3 = (f32[32,16,32,64]{3,2,1,0:T(8,128)}, f32[32,16,32,64]{3,2,1,0:T(8,128)}) fusion(f32[32,64,16]{1,2,0:T(8,128)S(1)} %get-tuple-element.375, f32[32,32]{1,0:T(8,128)S(1)} %copy.439, f32[32,64,16]{1,2,0:T(8,128)S(1)} %get-tuple-element.376), kind=kLoop, calls=%fused_computation.13 | loop fusion | flops 2097152 | bytes 8654848 | tf_op jit(solution)/shard_map/gnc,gh->gchn/transpose | solution.py:111
  17.9 7.8 reshape.265
  25.7 7.8 reshape.266
  33.5 8.2 %fusion.4 = f32[256,4096]{1,0:T(8,128)S(1)} fusion(bf16[256,512]{1,0:T(8,128)(2,1)S(1)} %copy-done.103, f32[512,2048]{1,0:T(8,128)} %reshape.266, f32[512,2048]{1,0:T(8,128)} %reshape.265), kind=kOutput, calls=%fused_computation.14 | convolution fusion | flops 6444548096 | bytes 12845056 | tf_op jit(solution)/shard_map/dot_general | solution.py:116
  50.1 5.2 add.1617
  55.3 3.2 broadcast_multiply_fusion
  65.4 5.5 multiply_add_fusion.4
  139.6 3.1 multiply_subtract_fusion.2
  214.0 7.7 stack.10
  221.8 7.7 stack.9
  229.5 6.8 fusion.77
  236.9 32.5 %all-gather.2 = bf16[8,1,2048]{2,1,0:T(2,128)(2,1)S(1)} all-gather(bf16[1,1,2048]{2,1,0:T(2,128)(2,1)S(1)} %slice_bitcast_fusion.1), channel_id=1, replica_groups=mesh['sp'=8,'tp'=4] {'sp'}, dimensions={0}, use_global_device_ids=true | all-gather | bytes 36864 | tf_op jit(solution)/shard_map/all_gather | solution.py:14
  290.3 7.6 stack.11
  297.8 7.0 fusion.76
  304.9 30.7 %all-gather.3 = bf16[8,1,2048]{2,1,0:T(2,128)(2,1)S(1)} all-gather(bf16[1,1,2048]{2,1,0:T(2,128)(2,1)S(1)} %slice_bitcast_fusion), channel_id=1, replica_groups=mesh['sp'=8,'tp'=4] {'sp'}, dimensions={0}, use_global_device_ids=true | all-gather | bytes 36864 | tf_op jit(solution)/shard_map/all_gather | solution.py:14
  335.6 30.5 %all-gather.1 = bf16[8,1,2048]{2,1,0:T(2,128)(2,1)S(1)} all-gather(bf16[1,1,2048]{2,1,0:T(2,128)(2,1)S(1)} %slice_bitcast_fusion.2), channel_id=1, replica_groups=mesh['sp'=8,'tp'=4] {'sp'}, dimensions={0}, use_global_device_ids=true | all-gather | bytes 36864 | tf_op jit(solution)/shard_map/all_gather | solution.py:14
  366.2 30.5 %all-gather = bf16[8,1,2048]{2,1,0:T(2,128)(2,1)S(1)} all-gather(bf16[1,1,2048]{2,1,0:T(2,128)(2,1)S(1)} %slice_bitcast_fusion.3), channel_id=1, replica_groups=mesh['sp'=8,'tp'=4] {'sp'}, dimensions={0}, use_global_device_ids=true | all-gather | bytes 36864 | tf_op jit(solution)/shard_map/all_gather | solution.py:14
  396.8 6.8 while.16
  403.8 8.1 multiply_bitcast_fusion
  411.9 7.8 reshape.269
  419.7 8.0 reshape.270
  427.7 5.5 multiply_add_fusion
  433.2 3.7 fusion.95
  436.9 3.8 fusion.25
  442.6 25.8 %reduce-scatter.3.cloned.1.call-done = bf16[64,2048]{1,0:T(8,128)(2,1)} async-done(((bf16[256,2048]{1,0:T(8,128)(2,1)}), bf16[64,2048]{1,0:T(8,128)(2,1)}) %reduce-scatter.3.cloned.1.call-update) | async-done | bytes 262160 | tf_op jit(solution)/shard_map/reduce_scatter | solution.py:186
  473.9 14.7 %all-gather.9.cloned.1.call-done = bf16[256,2048]{1,0:T(8,128)(2,1)} async-done(((bf16[64,2048]{1,0:T(8,128)(2,1)}), bf16[256,2048]{1,0:T(8,128)(2,1)}) %all-gather.9.cloned.1.call-update) | async-done | bytes 1048592 | tf_op jit(solution)/shard_map/all_gather | solution.py:194
  488.5 94.5 %all-gather.11.cloned.1.call-done = bf16[2048,1408]{1,0:T(8,128)(2,1)} async-done(((bf16[256,1408]{1,0:T(8,128)(2,1)}), bf16[2048,1408]{1,0:T(8,128)(2,1)}) %all-gather.11.cloned.1.call-update) | async-done | bytes 5767184 | tf_op jit(solution)/shard_map/all_gather | solution.py:196
  583.1 5.9 fusion.96
  589.0 86.7 %all-gather.13.cloned.1.call-done = bf16[2048,1408]{1,0:T(8,128)(2,1)} async-done(((bf16[256,1408]{1,0:T(8,128)(2,1)}), bf16[2048,1408]{1,0:T(8,128)(2,1)}) %all-gather.13.cloned.1.call-update) | async-done | bytes 5767184 | tf_op jit(solution)/shard_map/all_gather | solution.py:197
  675.6 92.6 %all-gather.15.cloned.1.call-done = bf16[2048,1408]{1,0:T(8,128)(2,1)} async-done(((bf16[256,1408]{1,0:T(8,128)(2,1)}), bf16[2048,1408]{1,0:T(8,128)(2,1)}) %all-gather.15.cloned.1.call-update) | async-done | bytes 5767184 | tf_op jit(solution)/shard_map/all_gather | solution.py:198
  768.2 9.1 %convolution_convert_fusion.1 = bf16[256,2048]{1,0:T(8,128)(2,1)} fusion(bf16[2048,1408]{1,0:T(8,128)(2,1)} %all-gather.15.cloned.1.call-done, bf16[256,2048]{1,0:T(8,128)(2,1)S(1)} %copy-done.125, bf16[2048,1408]{1,0:T(8,128)(2,1)} %all-gather.13.cloned.1.call-done, f32[256,1408]{1,0:T(8,128)} %fusion.96), kind=kOutput, calls=%fused_computation.18 | convolution fusion | flops 2955476992 | bytes 15073280 | tf_op jit(solution)/shard_map/dot_general | solution.py:205
  777.4 23.1 %reduce-scatter.5.cloned.1.call-done = bf16[64,2048]{1,0:T(8,128)(2,1)} async-done(((bf16[256,2048]{1,0:T(8,128)(2,1)}), bf16[64,2048]{1,0:T(8,128)(2,1)}) %reduce-scatter.5.cloned.1.call-update) | async-done | bytes 262160 | tf_op jit(solution)/shard_map/reduce_scatter | solution.py:204
  (503 shorter events, 195.3 us)
Async XLA Ops:
  6.5 434.2 %copy-start = (bf16[512,2048]{1,0:T(8,128)(2,1)S(1)}, bf16[512,2048]{1,0:T(8,128)(2,1)}, u32[]{:S(2)}) copy-start(bf16[512,2048]{1,0:T(8,128)(2,1)} %param.29) | copy-start | bytes 6291460
  6.5 461.9 %reduce-scatter.3.cloned.1.call-start = ((), (), s32[]{:S(2)}) async-start(), calls=%async_computation.2 | async-start | bytes 1310720 | tf_op jit(solution)/shard_map/reduce_scatter | solution.py:186
  192.1 18.7 %copy-start.74 = (f32[16,1,2048]{2,0,1:T(8,128)S(1)}, f32[16,1,2048]{2,0,1:T(8,128)}, u32[]{:S(2)}) copy-start(f32[16,1,2048]{2,0,1:T(8,128)} %get-tuple-element.252) | copy-start | bytes 393220
  192.9 18.7 %copy-start.73 = (f32[16,1,2048]{2,0,1:T(8,128)S(1)}, f32[16,1,2048]{2,0,1:T(8,128)}, u32[]{:S(2)}) copy-start(f32[16,1,2048]{2,0,1:T(8,128)} %get-tuple-element.250) | copy-start | bytes 393220
  193.7 18.7 %copy-start.72 = (f32[16,1,2048]{2,0,1:T(8,128)S(1)}, f32[16,1,2048]{2,0,1:T(8,128)}, u32[]{:S(2)}) copy-start(f32[16,1,2048]{2,0,1:T(8,128)} %get-tuple-element.248) | copy-start | bytes 393220
  193.7 19.5 %copy-start.71 = (f32[16,1,2048]{2,0,1:T(8,128)S(1)}, f32[16,1,2048]{2,0,1:T(8,128)}, u32[]{:S(2)}) copy-start(f32[16,1,2048]{2,0,1:T(8,128)} %get-tuple-element.246) | copy-start | bytes 393220
  195.1 18.9 %copy-start.29 = (f32[16,1,2048]{2,1,0:T(1,128)S(1)}, f32[16,1,2048]{2,1,0:T(1,128)}, u32[]{:S(2)}) copy-start(f32[16,1,2048]{2,1,0:T(1,128)} %get-tuple-element.328) | copy-start | bytes 393220
  195.1 18.9 %copy-start.81 = (f32[16,1,2048]{2,1,0:T(1,128)S(1)}, f32[16,1,2048]{2,1,0:T(1,128)}, u32[]{:S(2)}) copy-start(f32[16,1,2048]{2,1,0:T(1,128)} %copy.511) | copy-start | bytes 393220
  195.1 18.9 %copy-start.84 = (f32[16,1,2048]{2,1,0:T(1,128)S(1)}, f32[16,1,2048]{2,1,0:T(1,128)}, u32[]{:S(2)}) copy-start(f32[16,1,2048]{2,1,0:T(1,128)} %copy.520) | copy-start | bytes 393220
  236.3 33.8 %copy-start.104 = (f32[8,2048]{1,0:T(8,128)S(1)}, f32[8,2048]{1,0:T(8,128)}, u32[]{:S(2)}) copy-start(f32[8,2048]{1,0:T(8,128)} %add.1774) | copy-start | bytes 196612
  236.3 33.8 %copy-start.110 = (f32[7,2048]{1,0:T(8,128)S(1)}, f32[7,2048]{1,0:T(8,128)}, u32[]{:S(2)}) copy-start(f32[7,2048]{1,0:T(8,128)} %get-tuple-element.377) | copy-start | bytes 172036
  236.3 50.1 %copy-start.62 = (f32[16,1,2048]{2,0,1:T(8,128)S(1)}, f32[16,1,2048]{2,0,1:T(8,128)}, u32[]{:S(2)}) copy-start(f32[16,1,2048]{2,0,1:T(8,128)} %get-tuple-element.209) | copy-start | bytes 393220
  236.9 50.3 %copy-start.61 = (f32[16,1,2048]{2,0,1:T(8,128)S(1)}, f32[16,1,2048]{2,0,1:T(8,128)}, u32[]{:S(2)}) copy-start(f32[16,1,2048]{2,0,1:T(8,128)} %get-tuple-element.207) | copy-start | bytes 393220
  236.9 51.1 %copy-start.60 = (f32[16,1,2048]{2,0,1:T(8,128)S(1)}, f32[16,1,2048]{2,0,1:T(8,128)}, u32[]{:S(2)}) copy-start(f32[16,1,2048]{2,0,1:T(8,128)} %get-tuple-element.205) | copy-start | bytes 393220
  236.9 51.9 %copy-start.59 = (f32[16,1,2048]{2,0,1:T(8,128)S(1)}, f32[16,1,2048]{2,0,1:T(8,128)}, u32[]{:S(2)}) copy-start(f32[16,1,2048]{2,0,1:T(8,128)} %get-tuple-element.203) | copy-start | bytes 393220
  236.9 52.0 %copy-start.58 = (f32[16,1,2048]{2,0,1:T(8,128)S(1)}, f32[16,1,2048]{2,0,1:T(8,128)}, u32[]{:S(2)}) copy-start(f32[16,1,2048]{2,0,1:T(8,128)} %get-tuple-element.201) | copy-start | bytes 393220
  269.4 19.7 %copy-start.57 = (f32[16,1,2048]{2,0,1:T(8,128)S(1)}, f32[16,1,2048]{2,0,1:T(8,128)}, u32[]{:S(2)}) copy-start(f32[16,1,2048]{2,0,1:T(8,128)} %get-tuple-element.199) | copy-start | bytes 393220
  270.1 19.2 %copy-start.56 = (f32[16,1,2048]{2,0,1:T(8,128)S(1)}, f32[16,1,2048]{2,0,1:T(8,128)}, u32[]{:S(2)}) copy-start(f32[16,1,2048]{2,0,1:T(8,128)} %get-tuple-element.197) | copy-start | bytes 393220
  272.2 17.2 %copy-start.55 = (f32[16,1,2048]{2,0,1:T(8,128)S(1)}, f32[16,1,2048]{2,0,1:T(8,128)}, u32[]{:S(2)}) copy-start(f32[16,1,2048]{2,0,1:T(8,128)} %get-tuple-element.195) | copy-start | bytes 393220
  297.8 105.7 %copy-start.107 = (f32[32,16,64]{2,1,0:T(8,128)S(1)}, f32[32,16,64]{2,1,0:T(8,128)}, u32[]{:S(2)}) copy-start(f32[32,16,64]{2,1,0:T(8,128)} %param.26) | copy-start | bytes 393220
  304.9 98.8 %copy-start.108 = (f32[32,16,64]{2,1,0:T(8,128)S(1)}, f32[32,16,64]{2,1,0:T(8,128)}, u32[]{:S(2)}) copy-start(f32[32,16,64]{2,1,0:T(8,128)} %param.27) | copy-start | bytes 393220
  304.9 98.9 %copy-start.112 = (f32[32,32]{0,1:T(8,128)S(1)}, f32[32,32]{0,1:T(8,128)}, u32[]{:S(2)}) copy-start(f32[32,32]{0,1:T(8,128)} %copy-done.111) | copy-start | bytes 12292
  440.8 28.8 %copy-start.109 = (bf16[64,2048]{1,0:T(8,128)(2,1)S(1)}, bf16[64,2048]{1,0:T(8,128)(2,1)}, u32[]{:S(2)}) copy-start(bf16[64,2048]{1,0:T(8,128)(2,1)} %param.19) | copy-start | bytes 786436
  440.8 28.7 %copy-start.122 = (f32[2048]{0:T(1024)S(1)}, f32[2048]{0:T(1024)}, u32[]{:S(2)}) copy-start(f32[2048]{0:T(1024)} %param.30) | copy-start | bytes 24580
  440.8 30.0 %copy-start.123 = (f32[2048]{0:T(1024)S(1)}, f32[2048]{0:T(1024)}, u32[]{:S(2)}) copy-start(f32[2048]{0:T(1024)} %param.34) | copy-start | bytes 24580
  442.5 46.0 %all-gather.9.cloned.1.call-start = ((), (), s32[]{:S(2)}) async-start(), calls=%async_computation.3 | async-start | bytes 1310720 | tf_op jit(solution)/shard_map/all_gather | solution.py:194
  471.7 111.4 %all-gather.11.cloned.1.call-start = ((), (), s32[]{:S(2)}) async-start(), calls=%async_computation.4 | async-start | bytes 6488064 | tf_op jit(solution)/shard_map/all_gather | solution.py:196
  472.4 203.2 %all-gather.13.cloned.1.call-start = ((), (), s32[]{:S(2)}) async-start(), calls=%async_computation.5 | async-start | bytes 6488064 | tf_op jit(solution)/shard_map/all_gather | solution.py:197
  473.0 295.2 %all-gather.15.cloned.1.call-start = ((), (), s32[]{:S(2)}) async-start(), calls=%async_computation.6 | async-start | bytes 6488064 | tf_op jit(solution)/shard_map/all_gather | solution.py:198
  473.6 326.9 %reduce-scatter.5.cloned.1.call-start = ((), (), s32[]{:S(2)}) async-start(), calls=%async_computation.7 | async-start | bytes 1310720 | tf_op jit(solution)/shard_map/reduce_scatter | solution.py:204
  488.5 279.7 %copy-start.125 = (bf16[256,2048]{1,0:T(8,128)(2,1)S(1)}, bf16[256,2048]{1,0:T(8,128)(2,1)}, u32[]{:S(2)}) copy-start(bf16[256,2048]{1,0:T(8,128)(2,1)} %all-gather.9.cloned.1.call-done) | copy-start | bytes 3145732
  589.0 212.6 %copy-start.124 = (f32[2048]{0:T(1024)S(1)}, f32[2048]{0:T(1024)}, u32[]{:S(2)}) copy-start(f32[2048]{0:T(1024)} %param.35) | copy-start | bytes 24580
  (100 other events, 770.2 us)
Sparse Core Ops, SparseCore 0:
  442.7 25.6 reduce-scatter.2
  471.8 16.6 all-gather.8
  490.7 92.3 all-gather.10
  585.1 90.4 all-gather.12
  677.7 90.4 all-gather.14
  777.5 22.9 reduce-scatter.4
where the time goes:
time: 826 us; the launch traced here: 811 us
  waiting for transfers between devices  339 us (41%)
  local copies, waits for them, and re-layouts  201 us (24%)
  blocking collectives  124 us (15%)
  other arithmetic  97.4 us (12%)
  matrix products  32.5 us (4%)
  between operations  15.6 us (2%)
    all_gather x4, blocking collectives, carried_in(): lax.all_gather(part.astype(kind), axis)  124 us
    all_gather x1, waiting for transfers between devices, shards(): lax.all_gather(gate_weight, 'sp', axis=0, tiled=True)  94.5 us
    all_gather x1, waiting for transfers between devices, shards(): lax.all_gather(down_weight, 'sp', axis=0, tiled=True)  92.6 us
    all_gather x1, waiting for transfers between devices, shards(): lax.all_gather(up_weight, 'sp', axis=0, tiled=True)  86.7 us
    slice x43, local copies, waits for them, and re-layouts, blocked_scan(): inclusive = lax.associative_scan(chain_link, totals, axis=0)  57.2 us
    reduce_scatter x1, waiting for transfers between devices, shards(): lax.psum_scatter(jnp.dot(block, out_weight, preferred_element_type=jnp.fl...  25.8 us
    reduce_scatter x1, waiting for transfers between devices, shards(): lax.psum_scatter(lax.dot_general(block, down_full, (((1,), (1,)), ((), ()...  23.1 us
    another operation x3, local copies, waits for them, and re-layouts, blocked_scan(): jnp.stack([entry[part] for entry in collected], axis=1)  23 us
  transfers between devices with their start and end apart: 6, of which 6 were waited for; matrix products, arithmetic and copies ran while one was open for 1% of the time, Pallas kernels for 0%

commit v1 on v0

v1 whole, which is shorter than its diff:
```python
import functools

import jax
import jax.numpy as jnp
from jax import lax
from jax.experimental import pallas as pl
from jax.experimental.pallas import tpu as pltpu
from jax.sharding import PartitionSpec as P

EPSILON = 1e-06
CHUNKS = 8
LANES = 128
BLOCK = 512
MESH = pl.DeviceIdType.MESH


def rms_scale(values, gain):
    return values * lax.rsqrt(jnp.mean(values * values, axis=-1, keepdims=True) + EPSILON) * gain


def split(values):
    high = values.astype(jnp.bfloat16)
    return high, (values - high.astype(jnp.float32)).astype(jnp.bfloat16)


def dot32(a, b):
    return jnp.dot(a, b, preferred_element_type=jnp.float32)


def times(ar, ai, br, bi):
    return ar * br - ai * bi, ar * bi + ai * br


def greet(barrier, nt):
    place = lax.axis_index("tp")
    for d in range(1, nt):
        pl.semaphore_signal(
            barrier, inc=1, device_id={"tp": lax.rem(place + d, nt)}, device_id_type=MESH
        )


def own_rows(nt, rows):
    own = rows // nt
    return pl.ds(pl.multiple_of(lax.axis_index("tp") * own, own), own)


def scatter_rows(nt, part, landed, sems):
    place = lax.axis_index("tp")
    rows = part.shape[0]
    own = rows // nt
    copies = []
    for d in range(1, nt):
        peer = lax.rem(place + d, nt)
        copy = pltpu.make_async_remote_copy(
            src_ref=part.at[pl.ds(pl.multiple_of(peer * own, own), own)],
            dst_ref=landed.at[d - 1],
            send_sem=sems.at[0, d - 1],
            recv_sem=sems.at[1, d - 1],
            device_id={"tp": peer},
            device_id_type=MESH,
        )
        copy.start()
        copies.append(copy)
    total = part[own_rows(nt, rows), :].astype(jnp.float32)
    for d, copy in enumerate(copies):
        copy.wait()
        total = total + landed[d].astype(jnp.float32)
    return total


def ssm_kernel(
    n,
    nt,
    u,
    mag,
    cr,
    ci,
    er,
    ei,
    rr,
    ri,
    order,
    residual,
    weight,
    mix_gain,
    pre_gain,
    middle,
    out,
    dr,
    di,
    ends,
    send,
    recv,
    start,
    active,
    part,
    landed,
    rows_all,
    send_sem,
    recv_sem,
    tp_sem,
):
    me = lax.axis_index("sp")
    rows, flat = dr.shape
    steps = rows // CHUNKS
    packs, width, wide = er.shape
    block = min(BLOCK, flat)

    barrier = pltpu.get_barrier_semaphore()
    for d in range(1, n):
        pl.semaphore_signal(
            barrier, inc=1, device_id={"sp": lax.rem(me + d, n)}, device_id_type=MESH
        )
    greet(barrier, nt)
    for p in range(packs):
        piece = u[:, p * width : (p + 1) * width]
        for e, dst in ((er, dr), (ei, di)):
            high, low = split(e[p])
            dst[:, p * wide : (p + 1) * wide] = dot32(piece, high) + dot32(piece, low)

    for b in range(0, flat, block):
        at = pl.ds(b, block)
        kr = jnp.broadcast_to(cr[0:1, at], (CHUNKS, block))
        ki = jnp.broadcast_to(ci[0:1, at], (CHUNKS, block))

        def first(j, held):
            pr, pi, sr, si = held
            row = pl.ds(pl.multiple_of(j * CHUNKS, CHUNKS), CHUNKS)
            m = mag[row, at]
            ar, ai = m * kr, m * ki
            pr, pi = times(ar, ai, pr, pi)
            sr, si = times(ar, ai, sr, si)
            return pr, pi, sr + dr[row, at], si + di[row, at]

        zero = jnp.zeros((CHUNKS, block), jnp.float32)
        held = lax.fori_loop(0, steps, first, (zero + 1.0, zero, zero, zero), unroll=2)
        for k in range(4):
            ends[k, :, at] = held[k]

    pr, pi, sr, si = (ends[k, 0:1, :] for k in range(4))
    for c in range(1, CHUNKS):
        ar, ai, br, bi = (ends[k, c : c + 1, :] for k in range(4))
        pr, pi = times(ar, ai, pr, pi)
        sr, si = times(ar, ai, sr, si)
        sr, si = sr + br, si + bi
    for k, item in enumerate((pr, pi, sr, si)):
        send[k : k + 1, :] = item

    pl.semaphore_wait(barrier, n - 1 + nt - 1)
    copies = []
    for d in range(1, n):
        copy = pltpu.make_async_remote_copy(
            src_ref=send,
            dst_ref=recv.at[me],
            send_sem=send_sem.at[d - 1],
            recv_sem=recv_sem.at[d - 1],
            device_id={"sp": lax.rem(me + d, n)},
            device_id_type=MESH,
        )
        copy.start()
        copies.append(copy)
    for copy in copies:
        copy.wait()

    sr = jnp.zeros((1, flat), jnp.float32)
    si = sr
    for k in range(n - 1):
        ar, ai, br, bi = (recv[k, q : q + 1, :] for q in range(4))
        nr, ni = times(ar, ai, sr, si)
        sr = jnp.where(k < me, nr + br, sr)
        si = jnp.where(k < me, ni + bi, si)
    for c in range(CHUNKS):
        start[0, c : c + 1, :] = sr
        start[1, c : c + 1, :] = si
        ar, ai, br, bi = (ends[k, c : c + 1, :] for k in range(4))
        sr, si = times(ar, ai, sr, si)
        sr, si = sr + br, si + bi

    for b in range(0, flat, block):
        at = pl.ds(b, block)
        kr = jnp.broadcast_to(cr[0:1, at], (CHUNKS, block))
        ki = jnp.broadcast_to(ci[0:1, at], (CHUNKS, block))

        def second(j, held):
            row = pl.ds(pl.multiple_of(j * CHUNKS, CHUNKS), CHUNKS)
            m = mag[row, at]
            sr, si = times(m * kr, m * ki, *held)
            sr, si = sr + dr[row, at], si + di[row, at]
            dr[row, at] = sr
            di[row, at] = si
            return sr, si

        lax.fori_loop(0, steps, second, (start[0, :, at], start[1, :, at]), unroll=2)

    for p in range(packs):
        total = None
        for state, read in ((dr, rr), (di, ri)):
            high, low = split(state[:, p * wide : (p + 1) * wide])
            top, rest = split(read[p])
            term = dot32(high, top) + dot32(high, rest) + dot32(low, top)
            total = term if total is None else total + term
        active[:, p * width : (p + 1) * width] = jax.nn.gelu(total).astype(jnp.bfloat16)

    active[...] = dot32(order[...], active[...]).astype(jnp.bfloat16)
    columns = weight.shape[1]
    for b in range(0, columns, BLOCK):
        at = pl.ds(b, BLOCK)
        part[:, at] = dot32(active[...], weight[:, at]).astype(jnp.bfloat16)
    mixed = scatter_rows(nt, part, landed, tp_sem)
    inner = (residual[...].astype(jnp.float32) + rms_scale(mixed, mix_gain[...])).astype(
        jnp.bfloat16
    )
    middle[...] = inner
    own = own_rows(nt, rows)
    rows_all[own, :] = rms_scale(inner.astype(jnp.float32), pre_gain[...]).astype(jnp.bfloat16)
    copies = []
    for d in range(1, nt):
        copy = pltpu.make_async_remote_copy(
            src_ref=rows_all.at[own],
            dst_ref=rows_all.at[own],
            send_sem=tp_sem.at[2, d - 1],
            recv_sem=tp_sem.at[3, d - 1],
            device_id={"tp": lax.rem(lax.axis_index("tp") + d, nt)},
            device_id_type=MESH,
        )
        copy.start()
        copies.append(copy)
    for copy in copies:
        copy.wait()
    out[...] = rows_all[...]


def down_kernel(nt, hidden, weight, middle, gain, out, part, landed, tp_sem):
    barrier = pltpu.get_barrier_semaphore()
    greet(barrier, nt)
    for b in range(0, weight.shape[0], BLOCK):
        at = pl.ds(b, BLOCK)
        part[:, at] = lax.dot_general(
            hidden[...],
            weight[at, :],
            (((1,), (1,)), ((), ())),
            preferred_element_type=jnp.float32,
        ).astype(jnp.bfloat16)
    pl.semaphore_wait(barrier, nt - 1)
    total = scatter_rows(nt, part, landed, tp_sem)
    out[...] = (middle[...].astype(jnp.float32) + 0.5 * rms_scale(total, gain[...])).astype(
        jnp.bfloat16
    )


def branch(
    n,
    nt,
    inputs,
    pole_real,
    pole_imaginary,
    step_log,
    input_real,
    entry_map_quadrature,
    output_real,
    output_imaginary,
    added_log_decay,
    residual,
    out_weight,
    mix_gain,
    pre_gain,
):
    rows, channels = inputs.shape
    columns = out_weight.shape[1]
    groups, states = pole_real.shape
    width = input_real.shape[2]
    flat = groups * states
    step_size = jnp.exp(step_log)[:, None]
    log_size = pole_real * step_size
    angle = pole_imaginary * step_size
    cosine = jnp.cos(angle)
    sine = jnp.sin(angle)
    magnitude = jnp.exp(log_size)
    lift_real = jnp.expm1(log_size) * cosine - 2.0 * jnp.sin(0.5 * angle) ** 2
    lift_imaginary = magnitude * sine
    denominator = pole_real * pole_real + pole_imaginary * pole_imaginary
    ratio_real = (lift_real * pole_real + lift_imaginary * pole_imaginary) / denominator
    ratio_imaginary = (lift_imaginary * pole_real - lift_real * pole_imaginary) / denominator
    bar_real = (
        ratio_real[..., None] * input_real - ratio_imaginary[..., None] * entry_map_quadrature
    )
    bar_imaginary = (
        ratio_real[..., None] * entry_map_quadrature + ratio_imaginary[..., None] * input_real
    )
    pack = LANES // width
    packs = groups // pack
    same = jnp.eye(pack, dtype=jnp.float32)

    def entry(bar):
        bar = bar.reshape(packs, pack, states, width).transpose(0, 1, 3, 2)
        return (bar[:, :, :, None, :] * same[None, :, None, :, None]).reshape(
            packs, pack * width, pack * states
        )

    def read(weight):
        weight = weight.reshape(packs, pack, width, states).transpose(0, 1, 3, 2)
        return (weight[:, :, :, None, :] * same[None, :, None, :, None]).reshape(
            packs, pack * states, pack * width
        )

    def mixed_rows(values):
        return values.reshape(CHUNKS, rows // CHUNKS, -1).transpose(1, 0, 2).reshape(rows, -1)

    spread = jnp.repeat(mixed_rows(jnp.exp(added_log_decay)), states, axis=1)
    vmem = pl.BlockSpec(memory_space=pltpu.VMEM)
    place = jnp.arange(rows)
    order = jax.nn.one_hot(
        place % (rows // CHUNKS) * CHUNKS + place // (rows // CHUNKS), rows, dtype=jnp.bfloat16
    )
    return pl.pallas_call(
        functools.partial(ssm_kernel, n, nt),
        out_shape=(
            jax.ShapeDtypeStruct((rows // nt, columns), jnp.bfloat16),
            jax.ShapeDtypeStruct((rows, columns), jnp.bfloat16),
        ),
        in_specs=[vmem] * 13,
        out_specs=(vmem, vmem),
        scratch_shapes=[
            pltpu.VMEM((rows, flat), jnp.float32),
            pltpu.VMEM((rows, flat), jnp.float32),
            pltpu.VMEM((4, CHUNKS, flat), jnp.float32),
            pltpu.VMEM((CHUNKS, flat), jnp.float32),
            pltpu.VMEM((n, CHUNKS, flat), jnp.float32),
            pltpu.VMEM((2, CHUNKS, flat), jnp.float32),
            pltpu.VMEM((rows, channels), jnp.bfloat16),
            pltpu.VMEM((rows, columns), jnp.bfloat16),
            pltpu.VMEM((nt - 1, rows // nt, columns), jnp.bfloat16),
            pltpu.VMEM((rows, columns), jnp.bfloat16),
            pltpu.SemaphoreType.DMA((n - 1,)),
            pltpu.SemaphoreType.DMA((n - 1,)),
            pltpu.SemaphoreType.DMA((4, nt - 1)),
        ],
        cost_estimate=pl.CostEstimate(
            flops=24000000000, bytes_accessed=8000000, transcendentals=0
        ),
        compiler_params=pltpu.CompilerParams(
            collective_id=0, has_side_effects=True, vmem_limit_bytes=40 * 1024 * 1024
        ),
    )(
        mixed_rows(inputs),
        spread,
        (magnitude * cosine).reshape(1, flat),
        (magnitude * sine).reshape(1, flat),
        entry(bar_real),
        entry(bar_imaginary),
        read(output_real),
        read(-output_imaginary),
        order,
        residual,
        out_weight,
        mix_gain.reshape(1, columns),
        pre_gain.reshape(1, columns),
    )


def shards(
    n,
    nt,
    residual,
    ssm_input,
    pole_real,
    pole_imaginary,
    step_log,
    input_real,
    entry_map_quadrature,
    output_real,
    output_imaginary,
    added_log_decay,
    out_weight,
    mix_gain,
    gate_weight,
    up_weight,
    down_weight,
    pre_gain,
    post_gain,
):
    gate_full, up_full, down_full = (
        lax.all_gather(gate_weight, "sp", axis=0, tiled=True),
        lax.all_gather(up_weight, "sp", axis=0, tiled=True),
        lax.all_gather(down_weight, "sp", axis=0, tiled=True),
    )
    middle, mixer_input = branch(
        n,
        nt,
        ssm_input,
        pole_real,
        pole_imaginary,
        step_log,
        input_real,
        entry_map_quadrature,
        output_real,
        output_imaginary,
        added_log_decay,
        residual,
        out_weight,
        mix_gain,
        pre_gain,
    )
    gate_act = jnp.dot(mixer_input, gate_full, preferred_element_type=jnp.float32)
    up_act = jnp.dot(mixer_input, up_full, preferred_element_type=jnp.float32)
    hidden = (jax.nn.silu(gate_act) * up_act).astype(jnp.bfloat16)
    rows, columns = mixer_input.shape
    return pl.pallas_call(
        functools.partial(down_kernel, nt),
        out_shape=jax.ShapeDtypeStruct(residual.shape, jnp.bfloat16),
        in_specs=[pl.BlockSpec(memory_space=pltpu.VMEM)] * 4,
        out_specs=pl.BlockSpec(memory_space=pltpu.VMEM),
        scratch_shapes=[
            pltpu.VMEM((rows, columns), jnp.bfloat16),
            pltpu.VMEM((nt - 1, rows // nt, columns), jnp.bfloat16),
            pltpu.SemaphoreType.DMA((2, nt - 1)),
        ],
        cost_estimate=pl.CostEstimate(flops=8000000000, bytes_accessed=8000000, transcendentals=0),
        compiler_params=pltpu.CompilerParams(
            collective_id=1, has_side_effects=True, vmem_limit_bytes=24 * 1024 * 1024
        ),
    )(hidden, down_full, middle, post_gain.reshape(1, columns))


def solution(mesh):
    return jax.shard_map(
        functools.partial(shards, mesh.shape["sp"], mesh.shape["tp"]),
        mesh=mesh,
        in_specs=(
            P(("sp", "tp"), None),
            P("sp", "tp"),
            P("tp", None),
            P("tp", None),
            P("tp"),
            P("tp", None, None),
            P("tp", None, None),
            P("tp", None, None),
            P("tp", None, None),
            P("sp", "tp"),
            P("tp", None),
            P(),
            P("sp", "tp"),
            P("sp", "tp"),
            P("sp", "tp"),
            P(),
            P(),
        ),
        out_specs=P(("sp", "tp"), None),
        check_vma=False,
    )
```

time: 826 us -> 324 us (0.39); the launches traced: 811 us -> 324 us
  local copies, waits for them, and re-layouts: 201 us -> 22.8 us
  waiting for transfers between devices: 339 us -> 213 us
  blocking collectives: 124 us -> 0 us
  other arithmetic: 97.4 us -> 2.27 us
  Pallas kernels: 0 us -> 62.1 us
  matrix products: 32.5 us -> 10.4 us
    all_gather x4 -> x0, blocking collectives: 124 us -> none  [carried_in(): lax.all_gather(part.astype(kind), axis)]
    slice x52 -> x0, local copies, waits for them, and re-layouts: 71.9 us -> none  [the longest x43 57.2 us: blocked_scan(): inclusive = lax.associative_scan(chain_link, totals, axis=0)]
    pallas_call x0 -> x2, Pallas kernels: none -> 62.1 us  [the longest x1 48.6 us: branch(): pl.pallas_call(functools.partial(ssm_kernel, n, nt), out_shape=(jax.Shape...]
    all_gather x1, waiting for transfers between devices: 94.5 us -> 35.5 us  [shards(): lax.all_gather(gate_weight, 'sp', axis=0, tiled=True)]
    reduce_scatter x2 -> x0, waiting for transfers between devices: 48.9 us -> none  [the longest x1 25.8 us: shards(): lax.psum_scatter(jnp.dot(block, out_weight, preferred_element_type=jnp.fl...]
    add x32 -> x0, local copies, waits for them, and re-layouts: 37.5 us -> none  [the longest x15 17.6 us: chain_link(): next_real * decay_imaginary + next_imaginary * decay_real]
    reshape x4 -> x7, local copies, waits for them, and re-layouts: 31.5 us -> 3.45 us  [the longest x1 1.92 us: branch(): spread = jnp.repeat(mixed_rows(jnp.exp(added_log_decay)), states, axis=1)]
    add x30 -> x2, other arithmetic: 28 us -> 0.07 us  [the longest x1 0.06 us: branch(): ratio_real[..., None] * entry_map_quadrature]
  transfers between devices with their start and end apart: 6 -> 3, of which waited for: 6 -> 3; matrix products, arithmetic and copies ran while one was open for 1% -> 9% of each run, Pallas kernels for 0% -> 15%
where the time goes in v1:
time: 324 us
  waiting for transfers between devices  213 us (66%)
  Pallas kernels  62.1 us (19%)
  local copies, waits for them, and re-layouts  22.8 us (7%)
  between operations  13.4 us (4%)
  matrix products  10.4 us (3%)
    all_gather x1, waiting for transfers between devices, shards(): lax.all_gather(down_weight, 'sp', axis=0, tiled=True)  87.9 us
    all_gather x1, waiting for transfers between devices, shards(): lax.all_gather(up_weight, 'sp', axis=0, tiled=True)  87.2 us
    pallas_call x1, Pallas kernels, branch(): pl.pallas_call(functools.partial(ssm_kernel, n, nt), out_shape=(jax.Shape...  48.6 us
    all_gather x1, waiting for transfers between devices, shards(): lax.all_gather(gate_weight, 'sp', axis=0, tiled=True)  35.5 us
    pallas_call x1, Pallas kernels, shards(): pl.pallas_call(functools.partial(down_kernel, nt), out_shape=jax.ShapeDty...  13.5 us
    mul x9, local copies, waits for them, and re-layouts, read(): weight[:, :, :, None, :] * same[None, :, None, :, None]  9.86 us
  transfers between devices with their start and end apart: 3, of which 3 were waited for; matrix products, arithmetic and copies ran while one was open for 9% of the time, Pallas kernels for 15%

profile of v1, /device:TPU:0, one launch (start us, length us, event | category | flops | bytes accessed | tf_op | source)
XLA Modules:
  0.0 323.6 jit_solution(42444697057750321)
XLA Ops:
  6.6 0.7 all-gather.4.cloned.1.call-update
  7.3 0.7 all-gather.6.cloned.1.call-update
  8.1 0.7 all-gather.8.cloned.1.call-update
  8.8 0.2 fusion.2
  9.1 0.2 mul.199
  9.4 0.5 mul.200
  9.9 0.2 mul.207
  10.1 1.5 mul.208
  11.8 0.1 mul.202
  12.2 0.1 mul.213
  12.3 0.8 copy.26
  13.3 0.2 mul.216
  13.5 1.5 mul.217
  15.1 2.6 copy.29
  17.7 0.2 mul.210
  18.0 1.5 mul.211
  19.5 2.7 copy.27
  22.5 1.5 broadcast_in_dim.3
  24.0 1.9 copy.30.mag
  26.0 1.1 copy.32
  27.2 1.7 broadcast_multiply_fusion.2
  29.1 0.1 broadcast_multiply_fusion
  29.3 1.4 copy-done.1
  30.7 48.6 %shard_map.163 = (bf16[64,2048]{1,0:T(8,128)(2,1)S(1)}, bf16[256,2048]{1,0:T(8,128)(2,1)S(1)}) custom-call(bf16[256,512]{1,0:T(8,128)(2,1)S(1)} %bitcast.49, f32[256,2048]{1,0:T(8,128)S(1)} %copy.30.mag, f32[1,2048]{1,0:T(1,128)S(1)} %reshape.96.cr, f32[1,2048]{1,0:T(1,128)S(1)} %reshape.97.ci, f32[4,128,512]{2,1,0:T(8,128)S(1)} %get-tuple-element.14.er, ...), custom_call_target="tpu_custom_call" | custom-call | flops 24000000000 | bytes 8000000 | tf_op jit(solution)/shard_map/pallas_call | solution.py:315
  79.3 35.5 %all-gather.4.cloned.1.call-done = bf16[2048,1408]{1,0:T(8,128)(2,1)} async-done(((bf16[256,1408]{1,0:T(8,128)(2,1)}), bf16[2048,1408]{1,0:T(8,128)(2,1)}) %all-gather.4.cloned.1.call-update) | async-done | bytes 5767184 | tf_op jit(solution)/shard_map/all_gather | solution.py:383
  114.8 5.5 %fusion.10 = f32[256,1408]{1,0:T(8,128)} fusion(bf16[256,2048]{1,0:T(8,128)(2,1)S(1)} %get-tuple-element.7, bf16[2048,1408]{1,0:T(8,128)(2,1)} %all-gather.4.cloned.1.call-done), kind=kOutput, calls=%fused_computation.31 | convolution fusion | flops 1476395008 | bytes 8257536 | tf_op jit(solution)/shard_map/dot_general | solution.py:404
  120.3 87.2 %all-gather.6.cloned.1.call-done = bf16[2048,1408]{1,0:T(8,128)(2,1)} async-done(((bf16[256,1408]{1,0:T(8,128)(2,1)}), bf16[2048,1408]{1,0:T(8,128)(2,1)}) %all-gather.6.cloned.1.call-update) | async-done | bytes 5767184 | tf_op jit(solution)/shard_map/all_gather | solution.py:384
  207.5 4.9 %fusion.hidden = bf16[256,1408]{1,0:T(8,128)(2,1)S(1)} fusion(bf16[256,2048]{1,0:T(8,128)(2,1)S(1)} %get-tuple-element.7, bf16[2048,1408]{1,0:T(8,128)(2,1)} %all-gather.6.cloned.1.call-done, f32[256,1408]{1,0:T(8,128)} %fusion.10), kind=kOutput, calls=%fused_computation.1 | convolution fusion | flops 1478557696 | bytes 8978432 | tf_op jit(solution)/shard_map/dot_general | solution.py:405
  212.4 87.9 %all-gather.8.cloned.1.call-done.weight = bf16[2048,1408]{1,0:T(8,128)(2,1)} async-done(((bf16[256,1408]{1,0:T(8,128)(2,1)}), bf16[2048,1408]{1,0:T(8,128)(2,1)}) %all-gather.8.cloned.1.call-update) | async-done | bytes 5767184 | tf_op jit(solution)/shard_map/all_gather | solution.py:385
  300.2 2.6 copy-done
  302.9 13.5 %shard_map.164 = bf16[64,2048]{1,0:T(8,128)(2,1)S(1)} custom-call(bf16[256,1408]{1,0:T(8,128)(2,1)S(1)} %fusion.hidden, bf16[2048,1408]{1,0:T(8,128)(2,1)S(1)} %copy-done, bf16[64,2048]{1,0:T(8,128)(2,1)S(1)} %get-tuple-element.8.middle, f32[1,2048]{1,0:T(1,128)S(1)} %bitcast.52), custom_call_target="tpu_custom_call" | custom-call | flops 8000000000 | bytes 8000000 | tf_op jit(solution)/shard_map/pallas_call | solution.py:408
  316.4 0.7 copy.34
  (52 shorter events, 1.4 us)
Async XLA Ops:
  6.5 2.2 copy-start.16
  6.5 2.3 copy-start.15
  6.5 2.3 copy-start.14
  6.5 2.5 copy-start.11
  6.5 2.5 copy-start.12
  6.5 108.3 %all-gather.4.cloned.1.call-start = ((), (), s32[]{:S(2)}) async-start(), calls=%async_computation | async-start | bytes 6488064 | tf_op jit(solution)/shard_map/all_gather | solution.py:383
  7.3 200.2 %all-gather.6.cloned.1.call-start = ((), (), s32[]{:S(2)}) async-start(), calls=%async_computation.1 | async-start | bytes 6488064 | tf_op jit(solution)/shard_map/all_gather | solution.py:384
  8.0 292.2 %all-gather.8.cloned.1.call-start = ((), (), s32[]{:S(2)}) async-start(), calls=%async_computation.2 | async-start | bytes 6488064 | tf_op jit(solution)/shard_map/all_gather | solution.py:385
  11.6 1.6 copy-start.9
  15.1 2.6 copy-start.10
  18.0 4.2 %copy-start.13 = (f32[256,32]{0,1:T(8,128)S(1)}, f32[256,32]{0,1:T(8,128)}, u32[]{:S(2)}) copy-start(f32[256,32]{0,1:T(8,128)} %param.26) | copy-start | bytes 98308
  27.2 1.8 copy-start.6
  27.2 1.9 copy-start.7
  27.2 1.9 copy-start.8
  29.1 1.6 copy-start.1
  29.1 1.6 copy-start.2
  29.1 1.6 copy-start.3
  29.1 1.6 copy-start.4
  120.3 179.9 %copy-start.5 = (f32[2048]{0:T(1024)S(1)}, f32[2048]{0:T(1024)}, u32[]{:S(2)}) copy-start(f32[2048]{0:T(1024)} %param.33) | copy-start | bytes 24580
  300.2 2.6 copy-start
Sparse Core Ops, SparseCore 0:
  9.5 105.2 all-gather.3
  117.0 90.4 all-gather.5
  209.7 90.4 all-gather.7
